TPU v7x, 32 devices: a whole 2x2x4 slice. The times are simulated.
32 devices in a mesh: grp: 2 (over y), kv: 4 (over z), tp: 4 (over x, core).
Axes of the slice: x: 2, y: 2, z: 4, core: 2. Of those that a mesh axis runs over, the one named last changes fastest.
Arguments:
- tokens: bfloat16 [512, 8, 4096], P('kv', 'grp'), parts along dimension 1, may hold values from -72 to 72
- lengths: int32 [8], P('grp'), parts along dimension 0, may hold values from 1 to 512, 768 in all
- chosen: int32 [8, 32, 8, 8], P('grp', 'tp', 'kv'), parts along dimension 0, may hold values from -1 to 7, as said below
- w_query: bfloat16 [4096, 2048], P(None, 'tp'), may hold values from -0.09375 to 0.09375
- w_key: bfloat16 [4096, 2048], P(None, 'tp'), may hold values from -0.09375 to 0.09375
- w_value: bfloat16 [4096, 2048], P(None, 'tp'), may hold values from -0.09375 to 0.09375
- w_gate: bfloat16 [4096, 2, 32], P(None, None, 'tp'), may hold values from -0.09375 to 0.09375
- pool_weights: float32 [2, 32, 64], replicated, may hold values from -1 to 1
- w_out: bfloat16 [2048, 4096], P(None, 'tp'), may hold values from -0.5 to 0.5
Outputs:
- mixed: bfloat16 [512, 8, 4096], P(('kv', 'tp'), 'grp'), parts along dimension 1
There are 2 independent parts, one for each index of `grp`. A program takes and returns all parts, laid end to end along the dimension named above; an argument that names none is the same for every part. Nothing has to cross between parts.
Inputs may be any that keep to these rules, and one draw needn't show every extreme that they name: `chosen`: for query block b the live slots hold min(8, b+1) distinct blocks, all <= b, among them b, b-1 (when b >= 1) and 0; the other slots are -1.
All inputs are finite; a program needn't handle non-finite values.
Results may differ from a plain program's by a relative error of at most 0.014.
Values may be sent and summed in bfloat16 or wider, within the bound.
No kernel may reach another device: no remote copies, remote signals or barrier semaphores. Data moves between devices by JAX's collectives and lax.ppermute only.
A program may use at most 128 MiB of HBM per device.

v0:
```python
from functools import partial
import jax
import jax.numpy as jnp
from jax import lax
from jax.sharding import PartitionSpec as P

HD = 64
QB = 64
L_CMP = 32
LOW_FILL = -1e30


def pooled_blocks(key_rows, pool_weight):
    row_count, seq_count, head_count, head_dim = key_rows.shape
    grouped = key_rows.reshape(row_count // L_CMP, L_CMP, seq_count, head_count, head_dim)
    return (grouped * pool_weight[None, :, None, None, :]).sum(1).astype(jnp.bfloat16)


def pooled_attend(queries, key_pooled, val_pooled, query_pos, lengths):
    head_dim = queries.shape[-1]
    cmp_end = jnp.arange(key_pooled.shape[0]) * L_CMP + L_CMP - 1
    scores = jnp.einsum(
        "qshd,cshd->shqc", queries, key_pooled, preferred_element_type=jnp.float32
    ) * head_dim ** (-0.5)
    usable = (cmp_end[None, None, :] <= query_pos[None, :, None]) & (
        cmp_end[None, None, :] < lengths[:, None, None]
    )
    usable = usable[:, None]
    row_top = jnp.max(jnp.where(usable, scores, LOW_FILL), axis=-1, keepdims=True)
    weights = jnp.where(usable, jnp.exp(scores - row_top), 0.0)
    totals = jnp.sum(weights, axis=-1)
    gathered = jnp.einsum(
        "shqc,cshd->shqd",
        weights.astype(jnp.bfloat16),
        val_pooled,
        preferred_element_type=jnp.float32,
    )
    return gathered / jnp.where(totals > 0, totals, 1.0)[..., None]


def fold_step(running, key_piece, begin_row, queries, chosen, query_pos, lengths):
    maxima, totals, weighted = running
    piece_keys, piece_values = key_piece
    head_dim = queries.shape[-1]
    key_pos = jnp.arange(piece_keys.shape[0])
    key_blk = key_pos // QB
    picked = jnp.any(chosen[..., None] == key_blk, axis=3)
    picked = jnp.repeat(picked, QB, axis=2)
    usable = (
        picked
        & (key_pos[None, None, None, :] <= query_pos[None, None, :, None])
        & (key_pos[None, None, None, :] < lengths[:, None, None, None])
    )
    scores = jnp.einsum(
        "qshd,kshd->shqk", queries, piece_keys, preferred_element_type=jnp.float32
    ) * head_dim ** (-0.5)
    new_max = jnp.maximum(maxima, jnp.max(jnp.where(usable, scores, LOW_FILL), axis=-1))
    weights = jnp.where(usable, jnp.exp(scores - new_max[..., None]), 0.0)
    shrink = jnp.exp(maxima - new_max)
    totals = jnp.sum(weights, axis=-1)
    weighted = jnp.einsum(
        "shqk,kshd->shqd",
        weights.astype(jnp.bfloat16),
        piece_values,
        preferred_element_type=jnp.float32,
    )
    return (new_max, totals, weighted)


def body(tokens, lengths, chosen, w_query, w_key, w_value, w_gate, pool_weights, w_out):
    row_count, seq_count, model_width = tokens.shape
    head_count = w_query.shape[1] // HD
    query_pos = lax.axis_index("kv") * row_count + jnp.arange(row_count)
    flat_rows = tokens.reshape(row_count * seq_count, model_width)

    def project(weight):
        product = jnp.dot(flat_rows, weight, preferred_element_type=jnp.float32)
        return product.astype(jnp.bfloat16).reshape(row_count, seq_count, head_count, HD)

    queries = project(w_query)
    key_rows = project(w_key)
    value_rows = project(w_value)
    gate_values = jax.nn.sigmoid(
        jnp.dot(
            flat_rows,
            w_gate.reshape(model_width, 2 * head_count),
            preferred_element_type=jnp.float32,
        )
    )
    gate_values = gate_values.reshape(row_count, seq_count, 2, head_count)
    key_pooled, val_pooled = (
        lax.all_gather(pooled_blocks(key_rows, pool_weights[0]), "kv", axis=0, tiled=True),
        lax.all_gather(pooled_blocks(value_rows, pool_weights[1]), "kv", axis=0, tiled=True),
    )
    start_state = (
        jnp.full((seq_count, head_count, row_count), LOW_FILL, jnp.float32),
        jnp.zeros((seq_count, head_count, row_count), jnp.float32),
        jnp.zeros((seq_count, head_count, row_count, HD), jnp.float32),
    )
    step_fn = partial(
        fold_step, queries=queries, chosen=chosen, query_pos=query_pos, lengths=lengths
    )
    maxima, totals, weighted = step_fn(
        start_state,
        (
            lax.all_gather(key_rows, "kv", axis=0, tiled=True),
            lax.all_gather(value_rows, "kv", axis=0, tiled=True),
        ),
        jnp.int32(0),
    )
    picked_out = weighted / jnp.where(totals > 0, totals, 1.0)[..., None]
    pooled_out = pooled_attend(queries, key_pooled, val_pooled, query_pos, lengths)
    combined = gate_values[:, :, 0, :, None] * pooled_out.transpose(2, 0, 1, 3) + gate_values[
        :, :, 1, :, None
    ] * picked_out.transpose(2, 0, 1, 3)
    live = query_pos[:, None] < lengths[None, :]
    attended = (
        jnp.where(live[:, :, None, None], combined, 0.0)
        .astype(jnp.bfloat16)
        .reshape(row_count, seq_count, head_count * HD)
    )
    group_count = lax.axis_size("tp")
    all_heads = lax.all_gather(attended, "tp", axis=2, tiled=True)
    group_width = head_count * HD
    col_width = w_out.shape[1]
    grouped_rows = all_heads.reshape(row_count * seq_count, group_count, group_width)
    grouped_weight = w_out.reshape(group_count, group_width, col_width)
    partial_cols = jnp.einsum(
        "rgk,gkc->rgc", grouped_rows, grouped_weight, preferred_element_type=jnp.float32
    )
    column_sum = jnp.sum(partial_cols.astype(jnp.bfloat16).astype(jnp.float32), axis=1)
    column_out = column_sum.astype(jnp.bfloat16).reshape(row_count, seq_count, col_width)
    return lax.all_to_all(column_out, "tp", split_axis=0, concat_axis=2, tiled=True)


def solution(mesh):
    placed = (
        P("kv", "grp", None),
        P("grp"),
        P("grp", "tp", "kv", None),
        P(None, "tp"),
        P(None, "tp"),
        P(None, "tp"),
        P(None, None, "tp"),
        P(),
        P(None, "tp"),
    )
    return jax.shard_map(
        body, mesh=mesh, in_specs=placed, out_specs=P(("kv", "tp"), "grp", None), check_vma=False
    )
```

profile of v0, /device:TPU:0, one launch (start us, length us, event | category | flops | bytes accessed | tf_op | source)
XLA Modules:
  0.0 181.1 jit_solution(17314178159223339070)
XLA Ops:
  6.5 7.0 %reshape.216 = bf16[512,4096]{1,0:T(8,128)(2,1)} reshape(bf16[128,4,4096]{2,1,0:T(4,128)(2,1)} %param.9) | data formatting | bytes 8388608 | tf_op jit(solution)/shard_map/reshape | solution.py:74
  13.5 5.8 %convolution_convert_fusion.1 = bf16[512,512]{1,0:T(8,128)(2,1)S(1)} fusion(bf16[512,4096]{1,0:T(8,128)(2,1)} %reshape.216, bf16[4096,512]{1,0:T(8,128)(2,1)} %param.13), kind=kOutput, calls=%fused_computation.19 | convolution fusion | flops 2147745792 | bytes 8912896 | tf_op jit(solution)/shard_map/dot_general | solution.py:77
  19.3 0.5 reshape.221
  19.8 1.9 %copy.57 = bf16[128,4,8,64]{0,3,2,1:T(8,128)(2,1)} copy(bf16[128,4,8,64]{3,2,1,0:T(8,128)(2,1)S(1)} %reshape.221) | data formatting | bytes 1048576 | tf_op jit(solution)/shard_map/reshape | solution.py:78
  21.7 0.0 all-gather.6.cloned.1.call-start
  21.8 5.8 %convolution_convert_fusion = bf16[512,512]{1,0:T(8,128)(2,1)S(1)} fusion(bf16[512,4096]{1,0:T(8,128)(2,1)} %reshape.216, bf16[4096,512]{1,0:T(8,128)(2,1)} %param.14), kind=kOutput, calls=%fused_computation.18 | convolution fusion | flops 2147745792 | bytes 8912896 | tf_op jit(solution)/shard_map/dot_general | solution.py:77
  27.6 0.5 reshape.222
  28.1 1.9 %copy.59 = bf16[128,4,8,64]{0,3,2,1:T(8,128)(2,1)} copy(bf16[128,4,8,64]{3,2,1,0:T(8,128)(2,1)S(1)} %reshape.222) | data formatting | bytes 1048576 | tf_op jit(solution)/shard_map/reshape | solution.py:78
  30.1 0.2 all-gather.8.cloned.1.call-start
  30.3 1.8 %reshape.228 = f32[4,32,4,8,64]{4,3,2,1,0:T(8,128)} reshape(bf16[512,512]{1,0:T(8,128)(2,1)S(1)} %convolution_convert_fusion) | data formatting | bytes 1572864 | tf_op jit(solution)/shard_map/convert_element_type | solution.py:16
  32.1 0.4 reshape.227
  32.6 3.5 %fusion.17 = f32[512,16]{0,1:T(8,128)S(1)} fusion(bf16[512,4096]{1,0:T(8,128)(2,1)} %reshape.216, bf16[4096,2,8]{0,2,1:T(8,128)(2,1)S(1)} %copy-done), kind=kOutput, calls=%fused_computation.30 | convolution fusion | flops 67133440 | bytes 4358144 | tf_op jit(solution)/shard_map/dot_general | solution.py:84
  36.1 0.1 copy.51
  36.2 0.3 reshape.218
  36.5 0.4 fusion.29
  37.0 0.1 copy.52
  37.0 0.1 copy.56
  37.2 5.8 %convolution_convert_fusion.2 = bf16[512,512]{1,0:T(8,128)(2,1)S(1)} fusion(bf16[512,4096]{1,0:T(8,128)(2,1)} %reshape.216, bf16[4096,512]{1,0:T(8,128)(2,1)} %param.12), kind=kOutput, calls=%fused_computation.20 | convolution fusion | flops 2147745792 | bytes 8912896 | tf_op jit(solution)/shard_map/dot_general | solution.py:77
  43.0 1.5 reshape.219
  44.5 2.2 %copy.53 = bf16[128,4,8,64]{0,3,2,1:T(8,128)(2,1)S(1)} copy(bf16[128,4,8,64]{3,2,1,0:T(8,128)(2,1)} %reshape.219) | data formatting | bytes 1048576 | tf_op jit(solution)/shard_map/reshape | solution.py:78
  46.8 1.9 %multiply_reduce_fusion = bf16[4,4,8,64]{3,2,1,0:T(8,128)(2,1)S(1)} fusion(f32[4,32,4,8,64]{4,3,2,1,0:T(8,128)} %reshape.228, f32[32,64]{1,0:T(8,128)S(1)} %get-tuple-element.9), kind=kLoop, calls=%fused_computation.9 | loop fusion | flops 516096 | bytes 1073152 | tf_op jit(solution)/shard_map/reduce_sum | solution.py:16
  48.6 16.0 %all_gather.16 = bf16[16,4,8,64]{3,2,1,0:T(8,128)(2,1)S(1)} all-gather(bf16[4,4,8,64]{3,2,1,0:T(8,128)(2,1)S(1)} %multiply_reduce_fusion), channel_id=1, replica_groups=mesh['grp'=2,'kv'=4,'tp'=4] {'kv'}, dimensions={0}, use_global_device_ids=true | all-gather | bytes 81920 | tf_op jit(solution)/shard_map/all_gather | solution.py:93
  64.6 0.3 multiply_reduce_fusion.1
  64.9 18.8 %all_gather.15 = bf16[16,4,8,64]{3,2,1,0:T(8,128)(2,1)S(1)} all-gather(bf16[4,4,8,64]{3,2,1,0:T(8,128)(2,1)S(1)} %multiply_reduce_fusion.1), channel_id=1, replica_groups=mesh['grp'=2,'kv'=4,'tp'=4] {'kv'}, dimensions={0}, use_global_device_ids=true | all-gather | bytes 81920 | tf_op jit(solution)/shard_map/all_gather | solution.py:92
  83.7 0.5 compare_reduce_fusion
  84.2 0.1 broadcast_compare_fusion.1
  84.3 0.1 broadcast_compare_fusion.2
  84.3 0.1 iota_compare_fusion.1
  84.4 0.1 broadcast_compare_fusion
  84.5 0.1 broadcast_and_fusion
  84.6 0.3 convolution_multiply_fusion
  84.8 0.1 fusion.30
  85.0 0.1 iota_compare_fusion
  85.1 0.0 all-gather.4.cloned.1.call-done
  85.1 4.3 %select_reduce_fusion = (f32[4,8,128]{2,1,0:T(8,128)S(1)}, f32[4,8,128,512]{3,2,1,0:T(8,128)S(1)}) fusion(pred[4,512]{1,0:T(4,128)(4,1)S(1)} %iota_compare_fusion.1, pred[128,512]{1,0:T(8,128)(4,1)S(1)} %iota_compare_fusion, pred[4,8,2,512]{3,2,1,0:T(4,128)(4,1)S(1)} %compare_reduce_fusion, bf16[128,4,8,64]{0,3,2,1:T(8,128)(2,1)S(1)} %copy.53, ...), kind=kOutput, calls=%fused_computation.2 | convolution fusion | flops 278917120 | bytes 11126784 | tf_op jit(solution)/shard_map/qshd,kshd->shqk/dot_general | solution.py:54
  89.4 4.5 %fusion.2 = (f32[4,8,128]{2,1,0:T(8,128)S(1)}, bf16[4,8,128,512]{3,2,1,0:T(8,128)(2,1)}) fusion(f32[4,8,128,512]{3,2,1,0:T(8,128)S(1)} %get-tuple-element.12, f32[4,8,128]{2,1,0:T(8,128)S(1)} %broadcast_maximum_fusion, pred[4,512]{1,0:T(4,128)(4,1)S(1)} %iota_compare_fusion.1, pred[128,512]{1,0:T(8,128)(4,1)S(1)} %iota_compare_fusion, ...), kind=kLoop, calls=%fused_computation.5 | loop fusion | flops 14675968 | bytes 12716032 | tf_op jit(solution)/shard_map/reduce_sum | solution.py:60
  93.9 25.4 %all-gather.6.cloned.1.call-done = bf16[512,4,8,64]{0,3,2,1:T(8,128)(2,1)} async-done(((bf16[128,4,8,64]{0,3,2,1:T(8,128)(2,1)}), bf16[512,4,8,64]{0,3,2,1:T(8,128)(2,1)}) %all-gather.6.cloned.1.call-update) | async-done | bytes 2097168 | tf_op jit(solution)/shard_map/all_gather | solution.py:107
  119.3 4.4 %fusion.11 = f32[128,4,8,64]{0,3,2,1:T(8,128)S(1)} fusion(bf16[4,8,128,512]{3,2,1,0:T(8,128)(2,1)} %get-tuple-element.6, bf16[512,4,8,64]{0,3,2,1:T(8,128)(2,1)} %all-gather.6.cloned.1.call-done, f32[128,4,8]{0,2,1:T(8,128)S(1)} %compare_select_fusion, f32[128,4,8]{0,2,1:T(8,128)S(1)} %copy.56), kind=kOutput, calls=%fused_computation.22 | convolution fusion | flops 268959744 | bytes 7372800 | tf_op jit(solution)/shard_map/shqk,kshd->shqd/dot_general | solution.py:61
  123.7 0.4 fusion.9
  124.1 1.2 copy.60
  125.3 21.4 %all-gather.8.cloned.1.call-done = bf16[128,4,2048]{2,1,0:T(4,128)(2,1)} async-done(((bf16[128,4,512]{2,1,0:T(4,128)(2,1)}), bf16[128,4,2048]{2,1,0:T(4,128)(2,1)}) %all-gather.8.cloned.1.call-update) | async-done | bytes 2097168 | tf_op jit(solution)/shard_map/all_gather | solution.py:123
  146.7 3.1 %reshape.224 = bf16[512,4,512]{2,1,0:T(4,128)(2,1)S(1)} reshape(bf16[128,4,2048]{2,1,0:T(4,128)(2,1)} %all-gather.8.cloned.1.call-done) | data formatting | bytes 4194304 | tf_op jit(solution)/shard_map/reshape | solution.py:126
  149.9 4.6 %convert_reduce_fusion = bf16[512,1024]{1,0:T(8,128)(2,1)S(1)} fusion(bf16[4,512,1024]{2,1,0:T(8,128)(2,1)} %bitcast.66, bf16[512,4,512]{2,1,0:T(4,128)(2,1)S(1)} %reshape.224), kind=kOutput, calls=%fused_computation.7 | convolution fusion | flops 2151153664 | bytes 7340032 | tf_op jit(solution)/shard_map/rgk,gkc->rgc/dot_general | solution.py:128
  154.5 0.4 reshape.226
  154.9 16.9 %all_to_all.18 = bf16[128,4,1024]{2,1,0:T(4,128)(2,1)S(1)} all-to-all(bf16[128,4,1024]{2,1,0:T(4,128)(2,1)S(1)} %reshape.226), channel_id=1, replica_groups=mesh['grp'=2,'kv'=4,'tp'=4] {'tp'}, dimensions={0} | all-to-all | bytes 2097152 | tf_op jit(solution)/shard_map/all_to_all | solution.py:133
  171.8 0.3 copy.62
  172.1 0.8 copy.65
  172.9 1.6 reshape.229
  (21 shorter events, 0.1 us)
Async XLA Ops:
  6.5 26.1 %copy-start = (bf16[4096,2,8]{0,2,1:T(8,128)(2,1)S(1)}, bf16[4096,2,8]{0,2,1:T(8,128)(2,1)}, u32[]{:S(2)}) copy-start(bf16[4096,2,8]{0,2,1:T(8,128)(2,1)} %param.15) | copy-start | bytes 393220
  6.5 78.6 %all-gather.4.cloned.1.call-start = ((), (), s32[]{:S(2)}) async-start(), calls=%async_computation.1 | async-start | bytes 2621440 | tf_op jit(solution)/shard_map/all_gather | solution.py:106
  21.7 97.5 %all-gather.6.cloned.1.call-start = ((), (), s32[]{:S(2)}) async-start(), calls=%async_computation.2 | async-start | bytes 2621440 | tf_op jit(solution)/shard_map/all_gather | solution.py:107
  27.6 5.0 %copy-start.3 = (f32[2,32,64]{2,1,0:T(8,128)S(1)}, f32[2,32,64]{2,1,0:T(8,128)}, u32[]{:S(2)}) copy-start(f32[2,32,64]{2,1,0:T(8,128)} %param.16) | copy-start | bytes 49156
  30.1 116.6 %all-gather.8.cloned.1.call-start = ((), (), s32[]{:S(2)}) async-start(), calls=%async_computation.3 | async-start | bytes 2621440 | tf_op jit(solution)/shard_map/all_gather | solution.py:123
  43.0 40.7 %copy-start.2 = (s32[4,8,2,8]{3,2,1,0:T(2,128)S(1)}, s32[4,8,2,8]{3,2,1,0:T(2,128)}, u32[]{:S(2)}) copy-start(s32[4,8,2,8]{3,2,1,0:T(2,128)} %param.11) | copy-start | bytes 6148
  43.0 41.2 %copy-start.4 = (s32[4]{0:T(128)S(1)}, s32[4]{0:T(128)}, u32[]{:S(2)}) copy-start(s32[4]{0:T(128)} %param.10) | copy-start | bytes 52
  154.5 20.1 %copy-start.1 = (bf16[4096,2,8]{0,2,1:T(8,128)(2,1)S(1)}, bf16[4096,2,8]{0,2,1:T(8,128)(2,1)}, u32[]{:S(2)}) copy-start(bf16[4096,2,8]{0,2,1:T(8,128)(2,1)} %param.15) | copy-start | bytes 393220
Sparse Core Ops, SparseCore 0:
  21.9 51.1 all-gather.3
  74.6 44.6 all-gather.5
  125.4 21.2 all-gather.7
where the time goes:
time: 182 us; the launch traced here: 181 us
  blocking collectives  51.6 us (28%)
  waiting for transfers between devices  46.9 us (26%)
  matrix products  34.8 us (19%)
  local copies, waits for them, and re-layouts  26.4 us (15%)
  between operations  13.4 us (7%)
  other arithmetic  7.72 us (4%)
    all_gather x1, waiting for transfers between devices, body(): lax.all_gather(value_rows, 'kv', axis=0, tiled=True)  25.4 us
    all_gather x1, waiting for transfers between devices, body(): all_heads = lax.all_gather(attended, 'tp', axis=2, tiled=True)  21.4 us
    all_gather x1, blocking collectives, body(): lax.all_gather(pooled_blocks(key_rows, pool_weights[0]), 'kv', axis=0, ti...  18.8 us
    dot_general x3, matrix products, project(): product = jnp.dot(flat_rows, weight, preferred_element_type=jnp.float32)  17.4 us
    all_to_all x1, blocking collectives, body(): lax.all_to_all(column_out, 'tp', split_axis=0, concat_axis=2, tiled=True)  16.9 us
    all_gather x1, blocking collectives, body(): lax.all_gather(pooled_blocks(value_rows, pool_weights[1]), 'kv', axis=0,...  16 us
    reshape x6, local copies, waits for them, and re-layouts, project(): product.astype(jnp.bfloat16).reshape(row_count, seq_count, head_count, HD)  8.64 us
    reshape x1, local copies, waits for them, and re-layouts, body(): flat_rows = tokens.reshape(row_count * seq_count, model_width)  6.95 us
  transfers between devices with their start and end apart: 3, of which 2 were waited for; matrix products, arithmetic and copies ran while one was open for 20% of the time, Pallas kernels for 0%

commit v1 on v0

--- a/solution.py
+++ b/solution.py
@@ -120,7 +120,13 @@
         .reshape(row_count, seq_count, head_count * HD)
     )
     group_count = lax.axis_size("tp")
-    all_heads = lax.all_gather(attended, "tp", axis=2, tiled=True)
+    size = lax.axis_size("tp")
+    current, parts = (attended, [attended])
+    for _ in range(size - 1):
+        current = lax.ppermute(current, "tp", [(i, (i + 1) % size) for i in range(size)])
+        parts.insert(0, current)
+    line = jnp.concatenate(parts, axis=2)
+    all_heads = jnp.roll(line, (lax.axis_index("tp") + 1) * attended.shape[2], axis=2)
     group_width = head_count * HD
     col_width = w_out.shape[1]
     grouped_rows = all_heads.reshape(row_count * seq_count, group_count, group_width)

time: 182 us -> 189 us (1.038)
  waiting for transfers between devices: 46.9 us -> 51.1 us
    ppermute x0 -> x3, waiting for transfers between devices: none -> 25.8 us  [body(): lax.ppermute(current, 'tp', [(i, (i + 1) % size) for i in range(size)])]
    all_gather x1 -> x0, waiting for transfers between devices: 21.4 us -> none  [body(): all_heads = lax.all_gather(attended, 'tp', axis=2, tiled=True)]
  transfers between devices with their start and end apart: 3 -> 5, of which waited for: 2 -> 4; matrix products, arithmetic and copies ran while one was open for 20% -> 20% of each run, Pallas kernels for 0% -> 0%
where the time goes in v1:
time: 189 us; the launch traced here: 188 us
  blocking collectives  52 us (28%)
  waiting for transfers between devices  51.1 us (27%)
  matrix products  35.5 us (19%)
  local copies, waits for them, and re-layouts  28 us (15%)
  between operations  13.7 us (7%)
  other arithmetic  7.72 us (4%)
    ppermute x3, waiting for transfers between devices, body(): lax.ppermute(current, 'tp', [(i, (i + 1) % size) for i in range(size)])  25.8 us
    all_gather x1, waiting for transfers between devices, body(): lax.all_gather(value_rows, 'kv', axis=0, tiled=True)  25.3 us
    all_gather x1, blocking collectives, body(): lax.all_gather(pooled_blocks(key_rows, pool_weights[0]), 'kv', axis=0, ti...  19 us
    dot_general x3, matrix products, project(): product = jnp.dot(flat_rows, weight, preferred_element_type=jnp.float32)  17.4 us
    all_to_all x1, blocking collectives, body(): lax.all_to_all(column_out, 'tp', split_axis=0, concat_axis=2, tiled=True)  17 us
    all_gather x1, blocking collectives, body(): lax.all_gather(pooled_blocks(value_rows, pool_weights[1]), 'kv', axis=0,...  16 us
    reshape x6, local copies, waits for them, and re-layouts, project(): product.astype(jnp.bfloat16).reshape(row_count, seq_count, head_count, HD)  8.64 us
    reshape x1, local copies, waits for them, and re-layouts, body(): flat_rows = tokens.reshape(row_count * seq_count, model_width)  6.95 us
  transfers between devices with their start and end apart: 5, of which 4 were waited for; matrix products, arithmetic and copies ran while one was open for 20% of the time, Pallas kernels for 0%

profile of v1, /device:TPU:0, one launch (start us, length us, event | category | flops | bytes accessed | tf_op | source)
XLA Modules:
  0.0 188.3 jit_solution(14486756463867456871)
XLA Ops:
  6.5 7.0 %reshape.216 = bf16[512,4096]{1,0:T(8,128)(2,1)} reshape(bf16[128,4,4096]{2,1,0:T(4,128)(2,1)} %param.9) | data formatting | bytes 8388608 | tf_op jit(solution)/shard_map/reshape | solution.py:74
  13.5 5.8 %convolution_convert_fusion.1 = bf16[512,512]{1,0:T(8,128)(2,1)S(1)} fusion(bf16[512,4096]{1,0:T(8,128)(2,1)} %reshape.216, bf16[4096,512]{1,0:T(8,128)(2,1)} %param.13), kind=kOutput, calls=%fused_computation.19 | convolution fusion | flops 2147745792 | bytes 8912896 | tf_op jit(solution)/shard_map/dot_general | solution.py:77
  19.3 0.5 reshape.221
  19.8 1.9 %copy.63 = bf16[128,4,8,64]{0,3,2,1:T(8,128)(2,1)} copy(bf16[128,4,8,64]{3,2,1,0:T(8,128)(2,1)S(1)} %reshape.221) | data formatting | bytes 1048576 | tf_op jit(solution)/shard_map/reshape | solution.py:78
  21.7 0.2 all-gather.5.cloned.1.call-start
  22.0 5.8 %convolution_convert_fusion = bf16[512,512]{1,0:T(8,128)(2,1)S(1)} fusion(bf16[512,4096]{1,0:T(8,128)(2,1)} %reshape.216, bf16[4096,512]{1,0:T(8,128)(2,1)} %param.14), kind=kOutput, calls=%fused_computation.18 | convolution fusion | flops 2147745792 | bytes 8912896 | tf_op jit(solution)/shard_map/dot_general | solution.py:77
  27.8 0.5 reshape.222
  28.3 1.9 %copy.65 = bf16[128,4,8,64]{0,3,2,1:T(8,128)(2,1)} copy(bf16[128,4,8,64]{3,2,1,0:T(8,128)(2,1)S(1)} %reshape.222) | data formatting | bytes 1048576 | tf_op jit(solution)/shard_map/reshape | solution.py:78
  30.3 1.8 reshape.228
  32.1 0.4 reshape.227
  32.5 3.5 %fusion.17 = f32[512,16]{0,1:T(8,128)S(1)} fusion(bf16[512,4096]{1,0:T(8,128)(2,1)} %reshape.216, bf16[4096,2,8]{0,2,1:T(8,128)(2,1)S(1)} %copy-done), kind=kOutput, calls=%fused_computation.30 | convolution fusion | flops 67133440 | bytes 4358144 | tf_op jit(solution)/shard_map/dot_general | solution.py:84
  36.2 0.3 reshape.218
  36.5 0.4 fusion.29
  37.1 5.8 %convolution_convert_fusion.2 = bf16[512,512]{1,0:T(8,128)(2,1)S(1)} fusion(bf16[512,4096]{1,0:T(8,128)(2,1)} %reshape.216, bf16[4096,512]{1,0:T(8,128)(2,1)} %param.12), kind=kOutput, calls=%fused_computation.20 | convolution fusion | flops 2147745792 | bytes 8912896 | tf_op jit(solution)/shard_map/dot_general | solution.py:77
  43.0 1.5 reshape.219
  44.5 2.2 %copy.59 = bf16[128,4,8,64]{0,3,2,1:T(8,128)(2,1)S(1)} copy(bf16[128,4,8,64]{3,2,1,0:T(8,128)(2,1)} %reshape.219) | data formatting | bytes 1048576 | tf_op jit(solution)/shard_map/reshape | solution.py:78
  46.7 1.9 multiply_reduce_fusion
  48.6 16.0 %all_gather.13 = bf16[16,4,8,64]{3,2,1,0:T(8,128)(2,1)S(1)} all-gather(bf16[4,4,8,64]{3,2,1,0:T(8,128)(2,1)S(1)} %multiply_reduce_fusion), channel_id=1, replica_groups=mesh['grp'=2,'kv'=4,'tp'=4] {'kv'}, dimensions={0}, use_global_device_ids=true | all-gather | bytes 81920 | tf_op jit(solution)/shard_map/all_gather | solution.py:93
  64.6 0.3 multiply_reduce_fusion.1
  64.8 19.0 %all_gather.12 = bf16[16,4,8,64]{3,2,1,0:T(8,128)(2,1)S(1)} all-gather(bf16[4,4,8,64]{3,2,1,0:T(8,128)(2,1)S(1)} %multiply_reduce_fusion.1), channel_id=1, replica_groups=mesh['grp'=2,'kv'=4,'tp'=4] {'kv'}, dimensions={0}, use_global_device_ids=true | all-gather | bytes 81920 | tf_op jit(solution)/shard_map/all_gather | solution.py:92
  83.8 0.5 compare_reduce_fusion
  84.7 0.3 convolution_multiply_fusion
  85.0 0.1 fusion.30
  85.3 4.3 %select_reduce_fusion = (f32[4,8,128]{2,1,0:T(8,128)S(1)}, f32[4,8,128,512]{3,2,1,0:T(8,128)S(1)}) fusion(pred[4,512]{1,0:T(4,128)(4,1)S(1)} %iota_compare_fusion.1, pred[128,512]{1,0:T(8,128)(4,1)S(1)} %iota_compare_fusion, pred[4,8,2,512]{3,2,1,0:T(4,128)(4,1)S(1)} %compare_reduce_fusion, bf16[128,4,8,64]{0,3,2,1:T(8,128)(2,1)S(1)} %copy.59, ...), kind=kOutput, calls=%fused_computation.2 | convolution fusion | flops 278917120 | bytes 11126784 | tf_op jit(solution)/shard_map/qshd,kshd->shqk/dot_general | solution.py:54
  89.5 4.5 %fusion.2 = (f32[4,8,128]{2,1,0:T(8,128)S(1)}, bf16[4,8,128,512]{3,2,1,0:T(8,128)(2,1)}) fusion(f32[4,8,128,512]{3,2,1,0:T(8,128)S(1)} %get-tuple-element.12, f32[4,8,128]{2,1,0:T(8,128)S(1)} %broadcast_maximum_fusion, pred[4,512]{1,0:T(4,128)(4,1)S(1)} %iota_compare_fusion.1, pred[128,512]{1,0:T(8,128)(4,1)S(1)} %iota_compare_fusion, ...), kind=kLoop, calls=%fused_computation.5 | loop fusion | flops 14675968 | bytes 12716032 | tf_op jit(solution)/shard_map/reduce_sum | solution.py:60
  94.0 25.3 %all-gather.5.cloned.1.call-done = bf16[512,4,8,64]{0,3,2,1:T(8,128)(2,1)} async-done(((bf16[128,4,8,64]{0,3,2,1:T(8,128)(2,1)}), bf16[512,4,8,64]{0,3,2,1:T(8,128)(2,1)}) %all-gather.5.cloned.1.call-update) | async-done | bytes 2097168 | tf_op jit(solution)/shard_map/all_gather | solution.py:107
  119.3 4.4 %fusion.11 = f32[128,4,8,64]{0,3,2,1:T(8,128)S(1)} fusion(bf16[4,8,128,512]{3,2,1,0:T(8,128)(2,1)} %get-tuple-element.6, bf16[512,4,8,64]{0,3,2,1:T(8,128)(2,1)} %all-gather.5.cloned.1.call-done, f32[128,4,8]{0,2,1:T(8,128)S(1)} %compare_select_fusion, f32[128,4,8]{0,2,1:T(8,128)S(1)} %copy.62), kind=kOutput, calls=%fused_computation.22 | convolution fusion | flops 268959744 | bytes 7372800 | tf_op jit(solution)/shard_map/shqk,kshd->shqd/dot_general | solution.py:61
  123.7 0.4 fusion.9
  124.1 0.4 copy.66
  124.6 8.6 %collective-permute-done = bf16[128,4,512]{2,1,0:T(4,128)(2,1)S(1)} collective-permute-done((bf16[128,4,512]{2,1,0:T(4,128)(2,1)S(1)}, bf16[128,4,512]{2,1,0:T(4,128)(2,1)S(1)}, u32[]{:S(2)}, u32[]{:S(2)}) %collective-permute-start) | collective-permute-done | bytes 524320 | tf_op jit(solution)/shard_map/ppermute | solution.py:126
  133.2 8.6 %collective-permute-done.1 = bf16[128,4,512]{2,1,0:T(4,128)(2,1)S(1)} collective-permute-done((bf16[128,4,512]{2,1,0:T(4,128)(2,1)S(1)}, bf16[128,4,512]{2,1,0:T(4,128)(2,1)S(1)}, u32[]{:S(2)}, u32[]{:S(2)}) %collective-permute-start.1) | collective-permute-done | bytes 524320 | tf_op jit(solution)/shard_map/ppermute | solution.py:126
  141.8 8.6 %collective-permute-done.2 = bf16[128,4,512]{2,1,0:T(4,128)(2,1)S(1)} collective-permute-done((bf16[128,4,512]{2,1,0:T(4,128)(2,1)S(1)}, bf16[128,4,512]{2,1,0:T(4,128)(2,1)S(1)}, u32[]{:S(2)}, u32[]{:S(2)}) %collective-permute-start.2) | collective-permute-done | bytes 524320 | tf_op jit(solution)/shard_map/ppermute | solution.py:126
  150.4 0.3 constant_dynamic-update-slice_fusion.7
  150.7 0.2 constant_dynamic-update-slice_fusion.6
  150.9 0.2 constant_dynamic-update-slice_fusion.5
  151.2 0.2 constant_dynamic-update-slice_fusion.4
  151.4 0.2 constant_dynamic-update-slice_fusion.3
  151.6 0.2 constant_dynamic-update-slice_fusion.2
  151.9 0.2 constant_dynamic-update-slice_fusion.1
  152.1 0.2 constant_dynamic-update-slice_fusion
  152.4 1.0 constant_dynamic-slice_fusion
  153.4 2.7 %reshape.224 = bf16[512,4,512]{2,1,0:T(4,128)(2,1)} reshape(bf16[128,4,2048]{2,1,0:T(4,128)(2,1)S(1)} %constant_dynamic-slice_fusion) | data formatting | bytes 4194304 | tf_op jit(solution)/shard_map/reshape | solution.py:132
  156.0 5.3 %convert_reduce_fusion = bf16[512,1024]{1,0:T(8,128)(2,1)S(1)} fusion(bf16[4,512,1024]{2,1,0:T(8,128)(2,1)} %bitcast.66, bf16[512,4,512]{2,1,0:T(4,128)(2,1)} %reshape.224), kind=kOutput, calls=%fused_computation.7 | convolution fusion | flops 2151153664 | bytes 7340032 | tf_op jit(solution)/shard_map/rgk,gkc->rgc/dot_general | solution.py:134
  161.3 0.4 reshape.226
  161.7 17.0 %all_to_all.18 = bf16[128,4,1024]{2,1,0:T(4,128)(2,1)S(1)} all-to-all(bf16[128,4,1024]{2,1,0:T(4,128)(2,1)S(1)} %reshape.226), channel_id=1, replica_groups=mesh['grp'=2,'kv'=4,'tp'=4] {'tp'}, dimensions={0} | all-to-all | bytes 2097152 | tf_op jit(solution)/shard_map/all_to_all | solution.py:139
  178.7 0.3 copy.70
  179.1 0.8 copy.73
  179.9 1.6 reshape.229
  (33 shorter events, 1.0 us)
Async XLA Ops:
  6.5 26.0 %copy-start = (bf16[4096,2,8]{0,2,1:T(8,128)(2,1)S(1)}, bf16[4096,2,8]{0,2,1:T(8,128)(2,1)}, u32[]{:S(2)}) copy-start(bf16[4096,2,8]{0,2,1:T(8,128)(2,1)} %param.15) | copy-start | bytes 393220
  6.5 78.7 %all-gather.3.cloned.1.call-start = ((), (), s32[]{:S(2)}) async-start(), calls=%async_computation.1 | async-start | bytes 2621440 | tf_op jit(solution)/shard_map/all_gather | solution.py:106
  21.7 97.5 %all-gather.5.cloned.1.call-start = ((), (), s32[]{:S(2)}) async-start(), calls=%async_computation.2 | async-start | bytes 2621440 | tf_op jit(solution)/shard_map/all_gather | solution.py:107
  27.8 4.7 %copy-start.3 = (f32[2,32,64]{2,1,0:T(8,128)S(1)}, f32[2,32,64]{2,1,0:T(8,128)}, u32[]{:S(2)}) copy-start(f32[2,32,64]{2,1,0:T(8,128)} %param.16) | copy-start | bytes 49156
  42.9 40.9 %copy-start.2 = (s32[4,8,2,8]{3,2,1,0:T(2,128)S(1)}, s32[4,8,2,8]{3,2,1,0:T(2,128)}, u32[]{:S(2)}) copy-start(s32[4,8,2,8]{3,2,1,0:T(2,128)} %param.11) | copy-start | bytes 6148
  42.9 41.4 %copy-start.4 = (s32[4]{0:T(128)S(1)}, s32[4]{0:T(128)}, u32[]{:S(2)}) copy-start(s32[4]{0:T(128)} %param.10) | copy-start | bytes 52
  124.5 8.7 %collective-permute-start = (bf16[128,4,512]{2,1,0:T(4,128)(2,1)S(1)}, bf16[128,4,512]{2,1,0:T(4,128)(2,1)S(1)}, u32[]{:S(2)}, u32[]{:S(2)}) collective-permute-start(bf16[128,4,512]{2,1,0:T(4,128)(2,1)S(1)} %copy.66), channel_id=1, source_target_pairs={{0,1},{1,2},{2,3},{3,0},{4,5},{5,6},{6,7},{7,4},{8,9},{9,10},{10,1... | collective-permute-start | bytes 1572872 | tf_op jit(solution)/shard_map/ppermute | solution.py:126
  133.2 8.6 %collective-permute-start.1 = (bf16[128,4,512]{2,1,0:T(4,128)(2,1)S(1)}, bf16[128,4,512]{2,1,0:T(4,128)(2,1)S(1)}, u32[]{:S(2)}, u32[]{:S(2)}) collective-permute-start(bf16[128,4,512]{2,1,0:T(4,128)(2,1)S(1)} %collective-permute-done), channel_id=1, source_target_pairs={{0,1},{1,2},{2,3},{3,0},{4,5},{5,6},{6,7},{7,4},{8,9},{9,10},{10,1... | collective-permute-start | bytes 1572872 | tf_op jit(solution)/shard_map/ppermute | solution.py:126
  141.8 8.6 %collective-permute-start.2 = (bf16[128,4,512]{2,1,0:T(4,128)(2,1)S(1)}, bf16[128,4,512]{2,1,0:T(4,128)(2,1)S(1)}, u32[]{:S(2)}, u32[]{:S(2)}) collective-permute-start(bf16[128,4,512]{2,1,0:T(4,128)(2,1)S(1)} %collective-permute-done.1), channel_id=1, source_target_pairs={{0,1},{1,2},{2,3},{3,0},{4,5},{5,6},{6,7},{7,4},{8,9},{9,10},{10,1... | collective-permute-start | bytes 1572872 | tf_op jit(solution)/shard_map/ppermute | solution.py:126
  161.3 20.2 %copy-start.1 = (bf16[4096,2,8]{0,2,1:T(8,128)(2,1)S(1)}, bf16[4096,2,8]{0,2,1:T(8,128)(2,1)}, u32[]{:S(2)}) copy-start(bf16[4096,2,8]{0,2,1:T(8,128)(2,1)} %param.15) | copy-start | bytes 393220
Sparse Core Ops, SparseCore 0:
  21.9 51.5 all-gather.2
  75.0 44.2 all-gather.4
